TPU v7x, 32 devices: a whole 2x2x4 slice. The times are simulated.
32 devices in a mesh: grp: 2 (over y), st: 4 (over z), tp: 4 (over x, core).
Axes of the slice: x: 2, y: 2, z: 4, core: 2. Of those that a mesh axis runs over, the one named last changes fastest.
Arguments:
- pass_ids: int32 [64, 4], P(('grp', 'st')), parts along dimension 0, may hold values from 0 to 63, as said below
- store: bfloat16 [64, 64, 2048], P('st', None, 'tp'), may hold values from -6 to 6
- queries: bfloat16 [8192, 1024], P(('grp', 'st'), 'tp'), parts along dimension 0, may hold values from -40 to 40
- gate_pre: bfloat16 [8192, 1024], P(('grp', 'st'), 'tp'), parts along dimension 0, may hold values from -6 to 6
- w_query: bfloat16 [2048, 1024], P(None, 'tp'), may hold values from -0.125 to 0.125
- w_gate: bfloat16 [2048, 1024], P(None, 'tp'), may hold values from -0.125 to 0.125
- w_key: bfloat16 [2048, 1024], P(None, 'tp'), may hold values from -0.125 to 0.125
- w_value: bfloat16 [2048, 1024], P(None, 'tp'), may hold values from -0.125 to 0.125
- d_mem: bfloat16 [8192, 1024], P(('grp', 'st'), 'tp'), parts along dimension 0, may hold values from -6 to 6
Outputs:
- d_tokens: bfloat16 [8192, 2048], P(('grp', 'st', 'tp')), parts along dimension 0
- d_store: bfloat16 [128, 64, 2048], P(('grp', 'st', 'tp')), parts along dimension 0
- d_wkey: float32 [4096, 1024], P(('grp', 'st'), 'tp'), parts along dimension 0
There are 2 independent parts, one for each index of `grp`. A program takes and returns all parts, laid end to end along the dimension named above; an argument that names none is the same for every part. Nothing has to cross between parts.
Inputs may be any that keep to these rules, and one draw needn't show every extreme that they name: `pass_ids`: the 8 blocks of one index of st name at most 8 passages (counted with repetition) held by any one index of st o, that is passages o * 16 to o * 16 + 15. Every index of st takes exactly 8 passages from each of 4 indices of st and none from the others, so the bound 8 is reached by every index.
All inputs are finite; a program needn't handle non-finite values.
Results may differ from a plain program's by a relative error of at most 0.02.
Values may be sent and summed in bfloat16 or wider, within the bound.
A program may use at most 128 MiB of HBM per device.

v0:
```python
import jax
import jax.numpy as jnp
from jax import lax
from jax.sharding import PartitionSpec as P

HD = 256
BLK = 128
PB = 4


def local(pass_ids, store, queries, gate_pre, w_query, w_gate, w_key, w_value, d_mem):
    st_count = lax.axis_size("st")
    tp_count = lax.axis_size("tp")
    tok_rows, head_cols = queries.shape
    head_count = head_cols // HD
    blocks = tok_rows // BLK
    passages = store.shape[0]
    pass_len = store.shape[1]
    model_width = w_key.shape[0]
    requests = blocks * PB
    slot_depth = max(2, requests // st_count)
    slot_total = st_count * slot_depth
    pair_cols = 2 * head_cols
    request_ids = pass_ids.reshape(-1)
    owners = request_ids // passages
    owner_hot = (owners[:, None] == jnp.arange(st_count, dtype=jnp.int32)[None, :]).astype(
        jnp.int32
    )
    ranking = jnp.sum(jnp.cumsum(owner_hot, axis=0) * owner_hot, axis=1) - 1
    slot_index = owners * slot_depth + ranking
    slot_hot = slot_index[:, None] == jnp.arange(slot_total, dtype=jnp.int32)[None, :]
    all_requests = lax.all_gather(pass_ids, "st", axis=0, tiled=True).reshape(st_count, requests)
    is_mine = all_requests // passages == lax.axis_index("st")
    placed = jnp.cumsum(is_mine.astype(jnp.int32), axis=1) - 1
    slot_match = is_mine[:, :, None] & (
        placed[:, :, None] == jnp.arange(slot_depth, dtype=jnp.int32)[None, None, :]
    )
    asked_rows = jnp.max(
        jnp.where(slot_match, (all_requests % passages)[:, :, None], -1), axis=1
    ).reshape(-1)
    weight_kv = jnp.concatenate([w_key, w_value], axis=1)
    gathered = lax.all_gather(store, "tp", axis=2, tiled=True)
    flat_rows = gathered.reshape(passages * pass_len, model_width)
    kv_pass = jnp.dot(flat_rows, weight_kv, preferred_element_type=jnp.float32)
    kv_low = kv_pass.astype(jnp.bfloat16).reshape(passages, pass_len * pair_cols)
    pick_rows = (asked_rows[:, None] == jnp.arange(passages, dtype=jnp.int32)[None, :]).astype(
        jnp.bfloat16
    )
    outgoing = jnp.dot(pick_rows, kv_low, preferred_element_type=jnp.float32).astype(jnp.bfloat16)
    incoming = lax.all_to_all(
        outgoing.reshape(st_count, slot_depth, pass_len, pair_cols),
        "st",
        split_axis=0,
        concat_axis=0,
        tiled=True,
    )
    request_kv = incoming.reshape(slot_total, pass_len, pair_cols)[slot_index]
    block_kv = request_kv.reshape(blocks, PB * pass_len, pair_cols)
    key_rows = block_kv[:, :, :head_cols].reshape(blocks, PB * pass_len, head_count, HD)
    value_rows = block_kv[:, :, head_cols:].reshape(blocks, PB * pass_len, head_count, HD)
    query_rows = queries.reshape(blocks, BLK, head_count, HD)
    score_scale = HD ** (-0.5)
    scores = (
        jnp.einsum("nqhd,nkhd->nhqk", query_rows, key_rows, preferred_element_type=jnp.float32)
        * score_scale
    )
    shifted = jnp.exp(scores - jnp.max(scores, axis=-1, keepdims=True))
    prob_rows = shifted / jnp.sum(shifted, axis=-1, keepdims=True)
    probs_low = prob_rows.astype(jnp.bfloat16)
    attended = jnp.einsum(
        "nhqk,nkhd->nqhd", probs_low, value_rows, preferred_element_type=jnp.float32
    ).reshape(tok_rows, head_cols)
    gate_vals = gate_pre.astype(jnp.float32)
    sigmoid_vals = jax.nn.sigmoid(gate_vals)
    mem_grad = d_mem.astype(jnp.float32)
    attended_grad = (gate_vals * sigmoid_vals * mem_grad).astype(jnp.bfloat16)
    gate_grad = (
        mem_grad * attended * sigmoid_vals * (1.0 + gate_vals * (1.0 - sigmoid_vals))
    ).astype(jnp.bfloat16)
    attended_four = attended_grad.reshape(blocks, BLK, head_count, HD)
    prob_grad = jnp.einsum(
        "nqhd,nkhd->nhqk", attended_four, value_rows, preferred_element_type=jnp.float32
    )
    score_grad = (
        score_scale
        * prob_rows
        * (prob_grad - jnp.sum(prob_rows * prob_grad, axis=-1, keepdims=True))
    ).astype(jnp.bfloat16)
    query_grad = (
        jnp.einsum("nhqk,nkhd->nqhd", score_grad, key_rows, preferred_element_type=jnp.float32)
        .astype(jnp.bfloat16)
        .reshape(tok_rows, head_cols)
    )
    key_grad = jnp.einsum(
        "nhqk,nqhd->nkhd", score_grad, query_rows, preferred_element_type=jnp.float32
    )
    value_grad = jnp.einsum(
        "nhqk,nqhd->nkhd", probs_low, attended_four, preferred_element_type=jnp.float32
    )
    request_grads = jnp.concatenate(
        [
            key_grad.reshape(blocks, PB * pass_len, head_cols),
            value_grad.reshape(blocks, PB * pass_len, head_cols),
        ],
        axis=2,
    )
    request_grads = request_grads.astype(jnp.bfloat16).reshape(requests, pass_len * pair_cols)
    returning = jnp.dot(
        slot_hot.T.astype(jnp.bfloat16), request_grads, preferred_element_type=jnp.float32
    ).astype(jnp.bfloat16)
    arrived = lax.all_to_all(
        returning.reshape(st_count, slot_depth, pass_len, pair_cols),
        "st",
        split_axis=0,
        concat_axis=0,
        tiled=True,
    )
    pass_grad = jnp.dot(
        pick_rows.T,
        arrived.reshape(slot_total, pass_len * pair_cols),
        preferred_element_type=jnp.float32,
    )
    pass_low = pass_grad.astype(jnp.bfloat16).reshape(passages, pass_len, pair_cols)
    key_sums = pass_low[:, :, :head_cols].reshape(passages * pass_len, head_cols)
    d_wkey = lax.psum_scatter(
        jnp.einsum("rc,rh->ch", flat_rows, key_sums, preferred_element_type=jnp.float32),
        "st",
        scatter_dimension=0,
        tiled=True,
    )
    partial_value = pass_low.reshape(
        lax.axis_size("tp") * (passages // tp_count) * pass_len, pair_cols
    )
    d_store = lax.psum_scatter(
        jnp.einsum("rc,dc->rd", partial_value, weight_kv, preferred_element_type=jnp.float32)
        .reshape(lax.axis_size("tp") * (passages // tp_count), pass_len, model_width)
        .astype(jnp.bfloat16),
        "tp",
        scatter_dimension=0,
        tiled=True,
    )
    grad_both = jnp.concatenate([query_grad, gate_grad], axis=1)
    weight_both = jnp.concatenate([w_query, w_gate], axis=1)
    partial_value = grad_both
    d_tokens = lax.psum_scatter(
        jnp.einsum(
            "rc,dc->rd", partial_value, weight_both, preferred_element_type=jnp.float32
        ).astype(jnp.bfloat16),
        "tp",
        scatter_dimension=0,
        tiled=True,
    )
    return (d_tokens, d_store, d_wkey)


def solution(mesh):
    return jax.shard_map(
        local,
        mesh=mesh,
        in_specs=(
            P(("grp", "st"), None),
            P("st", None, "tp"),
            P(("grp", "st"), "tp"),
            P(("grp", "st"), "tp"),
            P(None, "tp"),
            P(None, "tp"),
            P(None, "tp"),
            P(None, "tp"),
            P(("grp", "st"), "tp"),
        ),
        out_specs=(
            P(("grp", "st", "tp"), None),
            P(("grp", "st", "tp"), None, None),
            P(("grp", "st"), "tp"),
        ),
        check_vma=False,
    )
```

profile of v0, /device:TPU:15, one launch (start us, length us, event | category | flops | bytes accessed | tf_op | source)
XLA Modules:
  0.0 335.5 jit_solution(900665779127207793)
XLA Ops:
  7.2 0.0 copy-start
  7.2 0.0 all-gather.3.cloned.1.call-start
  7.2 0.7 all-gather.3.cloned.1.call-update
  7.9 9.7 %all-gather = s32[4,8,4]{1,2,0:T(4,128)S(1)} all-gather(s32[1,8,4]{1,2,0:T(4,128)} %bitcast.77), channel_id=1, replica_groups=mesh['grp'=2,'st'=4,'tp'=4] {'st'}, dimensions={0}, use_global_device_ids=true | all-gather | bytes 640 | tf_op jit(solution)/shard_map/all_gather | solution.py:32
  17.6 0.1 copy.54
  17.7 0.1 reshape.320
  17.8 0.2 reduce_window_sum.22
  18.1 0.2 select_reduce_fusion.1
  18.2 0.1 eq.75
  18.3 2.4 constant_dynamic-update-slice_fusion.1
  20.7 1.1 constant_dynamic-update-slice_fusion
  21.8 22.8 %all-gather.3.cloned.1.call-done = bf16[16,64,2048]{2,1,0:T(8,128)(2,1)} async-done(((bf16[16,64,512]{2,1,0:T(8,128)(2,1)}), bf16[16,64,2048]{2,1,0:T(8,128)(2,1)}) %all-gather.3.cloned.1.call-update) | async-done | bytes 4194320 | tf_op jit(solution)/shard_map/all_gather | solution.py:42
  44.6 5.2 %fusion.6 = bf16[1024,512]{0,1:T(8,128)(2,1)S(1)} fusion(bf16[2048,512]{1,0:T(8,128)(2,1)} %constant_dynamic-update-slice_fusion, bf16[1024,2048]{1,0:T(8,128)(2,1)} %bitcast.78), kind=kOutput, calls=%fused_computation.20 | convolution fusion | flops 2148007936 | bytes 7340032 | tf_op jit(solution)/shard_map/dot_general | solution.py:44
  49.8 0.5 copy.55
  50.4 0.5 reshape.322
  50.9 0.7 convolution_convert_fusion.1
  51.7 2.1 copy.56
  53.7 4.7 %all-to-all-start = ((bf16[4,8,64,512]{3,2,1,0:T(8,128)(2,1)}), bf16[4,8,64,512]{3,2,1,0:T(8,128)(2,1)S(1)}, u32[]{:S(2)}, u32[]{:S(2)}) async-start(bf16[4,8,64,512]{3,2,1,0:T(8,128)(2,1)} %copy.56), calls=%async_computation | async-start | bytes 4194304 | tf_op jit(solution)/shard_map/all_to_all | solution.py:50
  58.4 0.1 copy.57
  58.5 0.1 reshape.326
  58.6 0.1 reshape.325
  58.7 0.1 fusion.30
  58.8 0.1 reduce_window_sum.23
  58.8 0.2 select_reduce_fusion
  59.1 44.1 %all-to-all-done = bf16[4,8,64,512]{3,2,1,0:T(8,128)(2,1)S(1)} async-done(((bf16[4,8,64,512]{3,2,1,0:T(8,128)(2,1)}), bf16[4,8,64,512]{3,2,1,0:T(8,128)(2,1)S(1)}, u32[]{:S(2)}, u32[]{:S(2)}) %all-to-all-start) | async-done | bytes 2097184 | tf_op jit(solution)/shard_map/all_to_all | solution.py:50
  103.2 1.3 copy-done.1
  104.5 2.3 gather_fusion
  106.8 0.4 fusion.9
  107.3 0.0 copy-start.3
  107.3 1.0 copy-done.3
  108.2 1.2 fusion.41
  109.4 3.1 fusion.21
  112.5 2.9 fusion.10
  115.4 3.3 fusion.7
  118.7 1.8 multiply_reduce_fusion
  120.5 0.2 multiply_convert_fusion
  120.6 0.5 convolution_convert_fusion.6
  121.1 0.5 copy-done.7
  121.7 1.5 pad_maximum_fusion
  123.2 4.0 %copy.67 = bf16[8,256,512]{2,1,0:T(8,128)(2,1)} copy(bf16[8,256,512]{1,2,0:T(8,128)(2,1)} %pad_maximum_fusion) | data formatting | bytes 4194304 | tf_op jit(solution)/shard_map/concatenate | solution.py:100
  127.1 4.3 %convert_element_type.82 = bf16[32,32768]{1,0:T(8,128)(2,1)} reshape(bf16[8,256,512]{2,1,0:T(8,128)(2,1)} %copy.67) | data formatting | bytes 4194304 | tf_op jit(solution)/shard_map/convert_element_type | solution.py:107
  131.4 2.4 convolution_convert_fusion
  133.9 50.8 %all_to_all.10 = bf16[4,8,64,512]{3,1,2,0:T(8,128)(2,1)S(1)} all-to-all(bf16[4,8,64,512]{3,1,2,0:T(8,128)(2,1)S(1)} %bitcast.68), channel_id=1, replica_groups=mesh['grp'=2,'st'=4,'tp'=4] {'st'}, dimensions={0} | all-to-all | bytes 4194304 | tf_op jit(solution)/shard_map/all_to_all | solution.py:111
  184.6 0.6 convolution_convert_fusion.2
  185.2 0.3 copy.76
  185.5 0.0 copy-start.5
  185.5 1.0 copy-done.5
  186.5 0.7 copy-done.12
  187.2 2.6 convolution_bitcast_fusion
  189.8 0.0 reduce-scatter.8.cloned.1.call-update
  189.8 0.0 reduce-scatter.4.cloned.1.call-start
  189.9 0.3 convolution_convert_fusion.8
  190.2 0.7 copy-done.9
  190.9 0.3 copy-done.13
  191.2 5.6 %convolution_convert_fusion.4 = bf16[1024,2048]{1,0:T(8,128)(2,1)} fusion(bf16[2048,256]{1,0:T(8,128)(2,1)S(1)} %copy-done.13, bf16[2048,256]{1,0:T(8,128)(2,1)} %param.13, bf16[1024,256]{1,0:T(8,128)(2,1)S(1)} %copy-done.9, bf16[1024,256]{1,0:T(8,128)(2,1)S(1)} %bitcast.76), kind=kOutput, calls=%fused_computation.6 | convolution fusion | flops 2155872256 | bytes 7340032 | tf_op jit(solution)/shard_map/rc,dc->rd/dot_general | solution.py:146
  196.9 0.0 reduce-scatter.4.cloned.1.call-update
  196.9 0.0 reduce-scatter.6.cloned.1.call-start
  196.9 1.1 copy-done.6
  198.1 6.1 %convolution_convert_fusion.3 = bf16[16,64,2048]{2,1,0:T(8,128)(2,1)} fusion(bf16[16,64,512]{2,1,0:T(8,128)(2,1)S(1)} %bitcast.73, bf16[2048,512]{1,0:T(8,128)(2,1)} %constant_dynamic-update-slice_fusion), kind=kOutput, calls=%fused_computation.5 | convolution fusion | flops 2149580800 | bytes 7340032 | tf_op jit(solution)/shard_map/rc,dc->rd/dot_general | solution.py:135
  204.2 0.0 reduce-scatter.6.cloned.1.call-update
  204.2 29.3 %reduce-scatter.8.cloned.1.call-done = f32[512,256]{0,1:T(8,128)} async-done(((f32[2048,256]{0,1:T(8,128)}), f32[512,256]{0,1:T(8,128)}) %reduce-scatter.8.cloned.1.call-update) | async-done | bytes 524304 | tf_op jit(solution)/shard_map/reduce_scatter | solution.py:125
  233.6 2.0 copy.68
  235.6 45.7 %reduce-scatter.4.cloned.1.call-done = bf16[256,2048]{1,0:T(8,128)(2,1)} async-done(((bf16[1024,2048]{1,0:T(8,128)(2,1)}), bf16[256,2048]{1,0:T(8,128)(2,1)}) %reduce-scatter.4.cloned.1.call-update) | async-done | bytes 1048592 | tf_op jit(solution)/shard_map/reduce_scatter | solution.py:145
  281.4 47.6 %reduce-scatter.6.cloned.1.call-done = bf16[4,64,2048]{2,1,0:T(8,128)(2,1)} async-done(((bf16[16,64,2048]{2,1,0:T(8,128)(2,1)}), bf16[4,64,2048]{2,1,0:T(8,128)(2,1)}) %reduce-scatter.6.cloned.1.call-update) | async-done | bytes 1048592 | tf_op jit(solution)/shard_map/reduce_scatter | solution.py:134
  (24 shorter events, 0.1 us)
Async XLA Ops:
  7.2 99.7 %copy-start = (bf16[1024,256]{1,0:T(8,128)(2,1)S(1)}, bf16[1024,256]{1,0:T(8,128)(2,1)}, u32[]{:S(2)}) copy-start(bf16[1024,256]{1,0:T(8,128)(2,1)} %param.11) | copy-start | bytes 1572868
  7.2 13.6 %copy-start.4 = (bf16[2048,256]{1,0:T(8,128)(2,1)S(1)}, bf16[2048,256]{1,0:T(8,128)(2,1)}, u32[]{:S(2)}) copy-start(bf16[2048,256]{1,0:T(8,128)(2,1)} %param.16) | copy-start | bytes 3145732
  7.2 37.4 %all-gather.3.cloned.1.call-start = ((), (), s32[]{:S(2)}) async-start(), calls=%async_computation.5 | async-start | bytes 5242880 | tf_op jit(solution)/shard_map/all_gather | solution.py:42
  53.7 4.7 %copy-start.11 = (s32[8,4]{0,1:T(4,128)S(1)}, s32[8,4]{0,1:T(4,128)}, u32[]{:S(2)}) copy-start(s32[8,4]{0,1:T(4,128)} %param.9) | copy-start | bytes 388
  53.7 49.5 %all-to-all-start = ((bf16[4,8,64,512]{3,2,1,0:T(8,128)(2,1)}), bf16[4,8,64,512]{3,2,1,0:T(8,128)(2,1)S(1)}, u32[]{:S(2)}, u32[]{:S(2)}) async-start(bf16[4,8,64,512]{3,2,1,0:T(8,128)(2,1)} %copy.56), calls=%async_computation | async-start | bytes 4194304 | tf_op jit(solution)/shard_map/all_to_all | solution.py:50
  58.4 175.1 %reduce-scatter.8.cloned.1.call-start = ((), (), s32[]{:S(2)}) async-start(), calls=%async_computation.8 | async-start | bytes 2621440 | tf_op jit(solution)/shard_map/reduce_scatter | solution.py:125
  103.2 1.3 copy-start.1
  107.3 1.0 copy-start.3
  109.4 3.1 copy-start.8
  115.4 3.3 copy-start.10
  118.7 1.8 copy-start.2
  120.4 1.2 copy-start.7
  184.6 2.6 copy-start.12
  185.5 1.0 copy-start.5
  189.8 91.6 %reduce-scatter.4.cloned.1.call-start = ((), (), s32[]{:S(2)}) async-start(), calls=%async_computation.6 | async-start | bytes 5242880 | tf_op jit(solution)/shard_map/reduce_scatter | solution.py:145
  189.9 1.0 copy-start.9
  189.9 1.4 copy-start.13
  196.9 1.2 copy-start.6
  196.9 132.0 %reduce-scatter.6.cloned.1.call-start = ((), (), s32[]{:S(2)}) async-start(), calls=%async_computation.7 | async-start | bytes 5242880 | tf_op jit(solution)/shard_map/reduce_scatter | solution.py:134
Sparse Core Ops, SparseCore 0:
  9.6 35.0 all-gather.2
  189.9 43.6 reduce-scatter.7
  236.7 44.6 reduce-scatter.3
  284.3 44.5 reduce-scatter.5
where the time goes:
time: 339 us; the launch traced here: 335 us
  waiting for transfers between devices  190 us (56%)
  blocking collectives  60.5 us (18%)
  matrix products  32.6 us (10%)
  local copies, waits for them, and re-layouts  26.7 us (8%)
  between operations  14 us (4%)
  other arithmetic  6.51 us (2%)
  starting transfers between devices  4.83 us (1%)
    all_to_all x1, blocking collectives, local(): lax.all_to_all(returning.reshape(st_count, slot_depth, pass_len, pair_col...  50.8 us
    reduce_scatter x1, waiting for transfers between devices, local(): lax.psum_scatter(jnp.einsum('rc,dc->rd', partial_value, weight_kv, prefer...  47.6 us
    reduce_scatter x1, waiting for transfers between devices, local(): lax.psum_scatter(jnp.einsum('rc,dc->rd', partial_value, weight_both, pref...  45.7 us
    all_to_all x1, waiting for transfers between devices, local(): lax.all_to_all(outgoing.reshape(st_count, slot_depth, pass_len, pair_cols...  44.1 us
    reduce_scatter x1, waiting for transfers between devices, local(): lax.psum_scatter(jnp.einsum('rc,rh->ch', flat_rows, key_sums, preferred_e...  29.3 us
    all_gather x1, waiting for transfers between devices, local(): gathered = lax.all_gather(store, 'tp', axis=2, tiled=True)  22.8 us
    unnamed x32, local copies, waits for them, and re-layouts  11.6 us
    all_gather x1, blocking collectives, local(): lax.all_gather(pass_ids, 'st', axis=0, tiled=True)  9.7 us
  transfers between devices with their start and end apart: 5, of which 5 were waited for; matrix products, arithmetic and copies ran while one was open for 6% of the time, Pallas kernels for 0%

commit v1 on v0

v1 whole, which is shorter than its diff:
```python
import functools

import jax
import jax.numpy as jnp
from jax import lax
from jax.experimental import pallas as pl
from jax.experimental.pallas import tpu as pltpu
from jax.sharding import PartitionSpec as P

HD = 256
BLK = 128
PB = 4
BF = jnp.bfloat16
F32 = jnp.float32
MESH = pl.DeviceIdType.MESH
NT = (((1,), (1,)), ((), ()))
TN = (((0,), (0,)), ((), ()))


def dot(a, b, dims=(((1,), (0,)), ((), ()))):
    return lax.dot_general(a, b, dims, preferred_element_type=F32)


def remote(src, dst, send, recv, device):
    return pltpu.make_async_remote_copy(
        src_ref=src,
        dst_ref=dst,
        send_sem=send,
        recv_sem=recv,
        device_id=device,
        device_id_type=MESH,
    )


def tile_of(size, most):
    while size % most:
        most //= 2
    return most


def kernel(
    st_n, tp_n, depth, pass_len,
    slot_ref, req_ref, ask_ref, store_ref, q_hbm, g_hbm, wq_hbm, wg_hbm, wk_hbm, wv_hbm, m_hbm,
    tok_out, store_out, wkey_out,
    rows, wkv, wqg, q_v, g_v, m_v, acc, kv, ask_in, ask_s, out, inc, kvb, reqg, gboth, arr,
    hot, plow, dwp, dwr, tp_part, tp_pair, tp_send, tp_recv, sp_part, sp_pair, sp_send, sp_recv,
    lsem, gs, gr, zs, zr, ps, pr, xs, xr,
):
    st = lax.axis_index("st")
    tp = lax.axis_index("tp")
    hi_n = tp_n // 2
    hi, lo = tp // 2, tp % 2
    mate = {"tp": hi * 2 + 1 - lo}
    pass_rows, chunk = rows.shape[1], rows.shape[2]
    model = wqg.shape[0]
    cols = q_v.shape[1]
    heads = cols // HD
    tok_rows = q_v.shape[0]
    blocks = tok_rows // BLK
    blk_keys = PB * pass_len

    def local(i, src, dst):
        copy = pltpu.make_async_copy(src, dst, lsem.at[i])
        copy.start()
        return copy

    own_rows = local(0, store_ref, rows.at[tp])
    loads_kv = [
        local(1, wk_hbm, wkv.at[:, pl.ds(0, cols)]),
        local(2, wv_hbm, wkv.at[:, pl.ds(cols, cols)]),
    ]
    loads_q = [local(3, q_hbm, q_v), local(4, g_hbm, g_v), local(5, m_hbm, m_v)]
    loads_qg = [
        local(6, wq_hbm, wqg.at[:, pl.ds(0, cols)]),
        local(7, wg_hbm, wqg.at[:, pl.ds(cols, cols)]),
    ]

    barrier = pltpu.get_barrier_semaphore()

    def greet_st(d, c):
        pl.semaphore_signal(
            barrier, inc=1, device_id={"st": (st + d) % st_n}, device_id_type=MESH
        )
        return c

    lax.fori_loop(1, st_n, greet_st, 0)
    for d in range(1, tp_n):
        pl.semaphore_signal(
            barrier, inc=1, device_id={"tp": (tp + d) % tp_n}, device_id_type=MESH
        )
    pl.semaphore_wait(barrier, st_n - 1 + tp_n - 1)

    across = []
    for d in range(1, hi_n):
        h = (hi + d) % hi_n
        across.append(
            remote(store_ref, rows.at[tp], gs.at[0, h], gr.at[tp], {"tp": h * 2 + lo})
        )
        across[-1].start()
    beside = remote(store_ref, rows.at[tp], gs.at[1, hi], gr.at[tp], mate)
    beside.start()

    def z_copy(phase, src, dst, peer):
        return remote(src, dst, zs.at[phase, peer], zr.at[phase, st], {"st": peer})

    def z_wait(phase, src, dst, peer):
        remote(src, dst, zs.at[phase, peer], zr.at[phase, peer], {"st": peer}).wait_recv()

    def ask_send(d, c):
        peer = (st + d) % st_n
        z_copy(0, ask_ref.at[peer], ask_in.at[st], peer).start()
        return c

    lax.fori_loop(1, st_n, ask_send, 0)
    ask_in[st] = ask_ref[st]

    m_tile = tile_of(pass_rows, 256)

    def project(t, first):
        def step(i, c):
            r = pl.ds(pl.multiple_of(i * m_tile, m_tile), m_tile)
            part = dot(rows[t, r], wkv[pl.ds(pl.multiple_of(t * chunk, chunk), chunk), :])
            acc[r] = part if first else acc[r] + part
            return c

        lax.fori_loop(0, pass_rows // m_tile, step, 0)

    def g_wait(t):
        remote(store_ref, rows.at[t], gs.at[1, hi], gr.at[t], mate).wait_recv()

    own_rows.wait()
    for copy in loads_kv:
        copy.wait()
    project(tp, True)
    g_wait(hi * 2 + 1 - lo)
    project(hi * 2 + 1 - lo, False)

    def ask_wait(d, c):
        peer = (st + d) % st_n
        z_wait(0, ask_ref.at[peer], ask_in.at[peer], peer)
        return c

    lax.fori_loop(1, st_n, ask_wait, 0)
    ask_copy = local(8, ask_in, ask_s)
    ask_copy.wait()

    hot_cols = depth * pass_len

    def hot_step(o, c):
        target = ask_in[o][0:1, :hot_cols]
        for i in range(pass_rows // m_tile):
            line = lax.broadcasted_iota(jnp.int32, (m_tile, hot_cols), 0) + i * m_tile
            hot[o, i * m_tile : (i + 1) * m_tile, :] = jnp.where(line == target, 1.0, 0.0).astype(BF)
        return c

    lax.fori_loop(0, st_n, hot_step, 0)
    onward = []
    for d in range(1, hi_n):
        h = (hi + d) % hi_n
        t = h * 2 + lo
        g_wait(t)
        onward.append(remote(rows.at[t], rows.at[t], gs.at[2, h], gr.at[t], mate))
        onward[-1].start()
        project(t, False)
    for d in range(1, hi_n):
        t = ((hi + d) % hi_n) * 2 + 1 - lo
        g_wait(t)
        project(t, False)

    def low_step(i, c):
        kv[i] = acc[pl.ds(pl.multiple_of(i * pass_len, pass_len), pass_len), :].astype(BF)
        return c

    lax.fori_loop(0, pass_rows // pass_len, low_step, 0)

    def kv_send(d, c):
        peer = (st + d) % st_n
        for k in range(depth):
            out[peer, k] = kv[ask_s[peer, 1, k]]
        z_copy(1, out.at[peer], inc.at[st], peer).start()
        return c

    lax.fori_loop(1, st_n, kv_send, 0)
    for k in range(depth):
        inc[st, k] = kv[ask_s[st, 1, k]]
    for copy in loads_q + loads_qg:
        copy.wait()

    def kv_wait(d, c):
        peer = (st + d) % st_n
        z_wait(1, out.at[peer], inc.at[peer], peer)
        return c

    lax.fori_loop(1, st_n, kv_wait, 0)

    scale = HD ** (-0.5)

    def block_step(b, c):
        r = pl.ds(pl.multiple_of(b * BLK, BLK), BLK)
        for j in range(PB):
            kvb[j * pass_len : (j + 1) * pass_len, :] = inc[
                slot_ref[0, b * PB + j], slot_ref[1, b * PB + j]
            ]
        for head in range(heads):
            hs = slice(head * HD, (head + 1) * HD)
            vs = slice(cols + head * HD, cols + (head + 1) * HD)
            q = q_v[r, hs]
            key = kvb[:, hs]
            value = kvb[:, vs]
            gate = g_v[r, hs].astype(F32)
            grad = m_v[r, hs].astype(F32)
            scores = dot(q, key, NT) * scale
            shifted = jnp.exp(scores - jnp.max(scores, axis=-1, keepdims=True))
            prob = shifted / jnp.sum(shifted, axis=-1, keepdims=True)
            low = prob.astype(BF)
            attended = dot(low, value)
            sig = 1.0 / (1.0 + jnp.exp(-gate))
            att_grad = (gate * sig * grad).astype(BF)
            gboth[r, vs] = (grad * attended * sig * (1.0 + gate * (1.0 - sig))).astype(BF)
            prob_grad = dot(att_grad, value, NT)
            inner = jnp.sum(prob * prob_grad, axis=-1, keepdims=True)
            score_grad = (scale * prob * (prob_grad - inner)).astype(BF)
            gboth[r, hs] = dot(score_grad, key).astype(BF)
            key_grad = dot(score_grad, q, TN).astype(BF)
            value_grad = dot(low, att_grad, TN).astype(BF)
            for j in range(PB):
                js = slice(j * pass_len, (j + 1) * pass_len)
                reqg[b * PB + j, :, hs] = key_grad[js]
                reqg[b * PB + j, :, vs] = value_grad[js]
        return c

    lax.fori_loop(0, blocks, block_step, 0)

    def grad_send(d, c):
        peer = (st + d) % st_n
        z_copy(1, out.at[peer], inc.at[st], peer).wait_send()
        for k in range(depth):
            out[peer, k] = reqg[req_ref[peer, k]]
        z_copy(2, out.at[peer], arr.at[st], peer).start()
        return c

    lax.fori_loop(1, st_n, grad_send, 0)
    for k in range(depth):
        arr[st, k] = reqg[req_ref[st, k]]

    n_tile = tile_of(model, 512)

    def expand(src, weight, part, pair_rows, t):
        base = pl.multiple_of(t * pair_rows, pair_rows)
        a = src[pl.ds(base, pair_rows), :]

        def step(i, c):
            n = pl.ds(pl.multiple_of(i * n_tile, n_tile), n_tile)
            part[t, :, n] = dot(a, weight[n, :], NT).astype(BF)
            return c

        lax.fori_loop(0, model // n_tile, step, 0)

    def pair_copy(which, part, pair, h):
        return remote(part.at[h * 2 + 1 - lo], pair.at[h], ps.at[which, h], pr.at[which, h], mate)

    def scatter_first(which, src, weight, part, pair, pair_rows):
        for d in range(1, hi_n + 1):
            h = (hi + d) % hi_n
            expand(src, weight, part, pair_rows, h * 2 + 1 - lo)
            pair_copy(which, part, pair, h).start()

    def cross(which, send, recv, h):
        return remote(
            send.at[h], recv.at[hi], xs.at[which, h], xr.at[which, hi], {"tp": h * 2 + lo}
        )

    def scatter_second(which, src, weight, part, pair, send, recv, pair_rows):
        for d in range(1, hi_n + 1):
            h = (hi + d) % hi_n
            expand(src, weight, part, pair_rows, h * 2 + lo)
            pair_copy(which, part, pair, h).wait_recv()
            if d < hi_n:
                send[h] = (part[h * 2 + lo].astype(F32) + pair[h].astype(F32)).astype(BF)
                cross(which, send, recv, h).start()

    def scatter_last(which, part, pair, send, recv, result):
        for d in range(1, hi_n):
            h = (hi + d) % hi_n
            remote(
                send.at[h], recv.at[h], xs.at[which, h], xr.at[which, h], {"tp": h * 2 + lo}
            ).wait_recv()
        total = part[tp].astype(F32) + pair[hi].astype(F32)
        for d in range(1, hi_n):
            total = total + recv[(hi + d) % hi_n].astype(F32)
        result[...] = total.astype(BF)

    tok_pair = tok_rows // tp_n
    sto_pair = pass_rows // tp_n
    scatter_first(0, gboth, wqg, tp_part, tp_pair, tok_pair)
    scatter_second(0, gboth, wqg, tp_part, tp_pair, tp_send, tp_recv, tok_pair)

    def grad_wait(d, c):
        peer = (st + d) % st_n
        z_wait(2, out.at[peer], arr.at[peer], peer)
        return c

    lax.fori_loop(1, st_n, grad_wait, 0)

    def sum_step(i, c):
        r = pl.ds(pl.multiple_of(i * m_tile, m_tile), m_tile)

        def owner(o, total):
            return total + dot(hot[o, r, :], arr[o].reshape(hot_cols, 2 * cols))

        total = lax.fori_loop(0, st_n, owner, jnp.zeros((m_tile, 2 * cols), F32))
        plow[r] = total.astype(BF)
        return c

    lax.fori_loop(0, pass_rows // m_tile, sum_step, 0)

    scatter_first(1, plow, wkv, sp_part, sp_pair, sto_pair)

    def wkey_step(t, c):
        dwp[pl.ds(pl.multiple_of(t * chunk, chunk), chunk), :] = dot(
            rows[t], plow[:, :cols], TN
        ).astype(BF)
        return c

    lax.fori_loop(0, tp_n, wkey_step, 0)
    share = model // st_n

    def part_of(s):
        return dwp.at[pl.ds(pl.multiple_of(s * share, share), share), :]

    def wkey_send(d, c):
        peer = (st + d) % st_n
        z_copy(3, part_of(peer), dwr.at[st], peer).start()
        return c

    lax.fori_loop(1, st_n, wkey_send, 0)
    scatter_second(1, plow, wkv, sp_part, sp_pair, sp_send, sp_recv, sto_pair)
    scatter_last(0, tp_part, tp_pair, tp_send, tp_recv, tok_out)
    wkey_out[...] = part_of(st)[...].astype(F32)

    def wkey_wait(d, c):
        peer = (st + d) % st_n
        z_wait(3, part_of(peer), dwr.at[peer], peer)
        wkey_out[...] += dwr[peer].astype(F32)
        return c

    lax.fori_loop(1, st_n, wkey_wait, 0)
    scatter_last(1, sp_part, sp_pair, sp_send, sp_recv, store_out)

    for copy in across + [beside] + onward:
        copy.wait_send()

    def drain(d, c):
        peer = (st + d) % st_n
        z_copy(0, ask_ref.at[peer], ask_in.at[st], peer).wait_send()
        z_copy(2, out.at[peer], arr.at[st], peer).wait_send()
        z_copy(3, part_of(peer), dwr.at[st], peer).wait_send()
        return c

    lax.fori_loop(1, st_n, drain, 0)
    for d in range(1, hi_n + 1):
        h = (hi + d) % hi_n
        pair_copy(0, tp_part, tp_pair, h).wait_send()
        pair_copy(1, sp_part, sp_pair, h).wait_send()
        if d < hi_n:
            cross(0, tp_send, tp_recv, h).wait_send()
            cross(1, sp_send, sp_recv, h).wait_send()


def local(pass_ids, store, queries, gate_pre, w_query, w_gate, w_key, w_value, d_mem):
    st_n = lax.axis_size("st")
    tp_n = lax.axis_size("tp")
    hi_n = tp_n // 2
    tok_rows, cols = queries.shape
    blocks = tok_rows // BLK
    passages, pass_len, chunk = store.shape
    model = w_key.shape[0]
    requests = blocks * PB
    depth = max(2, requests // st_n)
    pass_rows = passages * pass_len
    share = model // st_n

    ids = pass_ids.reshape(-1)
    owners = ids // passages
    within = ids % passages
    order = jnp.arange(requests, dtype=jnp.int32)
    earlier = (owners[None, :] == owners[:, None]) & (order[None, :] < order[:, None])
    rank = jnp.sum(earlier.astype(jnp.int32), axis=1)
    slots = jnp.stack([owners, rank])
    o_i = jnp.arange(st_n, dtype=jnp.int32)[:, None, None]
    k_i = jnp.arange(depth, dtype=jnp.int32)[None, :, None]
    match = (owners[None, None, :] == o_i) & (rank[None, None, :] == k_i)
    asked = jnp.max(jnp.where(match, within[None, None, :], -1), axis=2)
    req_of = jnp.max(jnp.where(match, order[None, None, :], 0), axis=2)
    hot_cols = depth * pass_len
    width = -(-hot_cols // 128) * 128
    lane = jnp.arange(width, dtype=jnp.int32)
    spread = jnp.repeat(asked, pass_len, axis=1)
    spread = jnp.pad(spread, ((0, 0), (0, width - hot_cols)), constant_values=-1)
    target = jnp.where(spread < 0, -1, spread * pass_len + lane[None, :] % pass_len)
    flat = jnp.pad(jnp.maximum(asked, 0), ((0, 0), (0, width - depth)))
    ask = jnp.concatenate(
        [target[:, None], flat[:, None], jnp.zeros((st_n, 6, width), jnp.int32)], axis=1
    )

    vmem = pl.BlockSpec(memory_space=pltpu.VMEM)
    smem = pl.BlockSpec(memory_space=pltpu.SMEM)
    hbm = pl.BlockSpec(memory_space=pl.ANY)
    V = pltpu.VMEM
    DMA = pltpu.SemaphoreType.DMA
    pair = 2 * cols
    tok_pair = tok_rows // tp_n
    sto_pair = pass_rows // tp_n
    d_tokens, d_store, d_wkey = pl.pallas_call(
        functools.partial(kernel, st_n, tp_n, depth, pass_len),
        out_shape=(
            jax.ShapeDtypeStruct((tok_pair, model), BF),
            jax.ShapeDtypeStruct((sto_pair, model), BF),
            jax.ShapeDtypeStruct((share, cols), F32),
        ),
        in_specs=[smem, smem, vmem] + [hbm] * 8,
        out_specs=(vmem, vmem, vmem),
        scratch_shapes=[
            V((tp_n, pass_rows, chunk), BF),
            V((model, pair), BF),
            V((model, pair), BF),
            V((tok_rows, cols), BF),
            V((tok_rows, cols), BF),
            V((tok_rows, cols), BF),
            V((pass_rows, pair), F32),
            V((passages, pass_len, pair), BF),
            V((st_n, 8, width), jnp.int32),
            pltpu.SMEM((st_n, 8, width), jnp.int32),
            V((st_n, depth, pass_len, pair), BF),
            V((st_n, depth, pass_len, pair), BF),
            V((PB * pass_len, pair), BF),
            V((requests, pass_len, pair), BF),
            V((tok_rows, pair), BF),
            V((st_n, depth, pass_len, pair), BF),
            V((st_n, pass_rows, hot_cols), BF),
            V((pass_rows, pair), BF),
            V((model, cols), BF),
            V((st_n, share, cols), BF),
            V((tp_n, tok_pair, model), BF),
            V((hi_n, tok_pair, model), BF),
            V((hi_n, tok_pair, model), BF),
            V((hi_n, tok_pair, model), BF),
            V((tp_n, sto_pair, model), BF),
            V((hi_n, sto_pair, model), BF),
            V((hi_n, sto_pair, model), BF),
            V((hi_n, sto_pair, model), BF),
            DMA((9,)),
            DMA((3, hi_n)),
            DMA((tp_n,)),
            DMA((4, st_n)),
            DMA((4, st_n)),
            DMA((2, hi_n)),
            DMA((2, hi_n)),
            DMA((2, hi_n)),
            DMA((2, hi_n)),
        ],
        compiler_params=pltpu.CompilerParams(
            collective_id=0, has_side_effects=True, vmem_limit_bytes=67043328
        ),
    )(
        slots, req_of, ask, store.reshape(pass_rows, chunk),
        queries, gate_pre, w_query, w_gate, w_key, w_value, d_mem,
    )
    return d_tokens, d_store.reshape(passages // tp_n, pass_len, model), d_wkey


def solution(mesh):
    return jax.shard_map(
        local,
        mesh=mesh,
        in_specs=(
            P(("grp", "st"), None),
            P("st", None, "tp"),
            P(("grp", "st"), "tp"),
            P(("grp", "st"), "tp"),
            P(None, "tp"),
            P(None, "tp"),
            P(None, "tp"),
            P(None, "tp"),
            P(("grp", "st"), "tp"),
        ),
        out_specs=(
            P(("grp", "st", "tp"), None),
            P(("grp", "st", "tp"), None, None),
            P(("grp", "st"), "tp"),
        ),
        check_vma=False,
    )
```

time: 339 us -> 191 us (0.56)
  the two profiles are of different devices: /device:TPU:15 before, /device:TPU:24 now
where the time goes in v1:
time: 191 us
  Pallas kernels  182 us (95%)
  local copies, waits for them, and re-layouts  5.83 us (3%)
  other arithmetic  2.32 us (1%)
    pallas_call x1, Pallas kernels, local(): pl.pallas_call(functools.partial(kernel, st_n, tp_n, depth, pass_len), ou...  182 us
    unnamed x10, local copies, waits for them, and re-layouts  5.26 us

profile of v1, /device:TPU:24, one launch (start us, length us, event | category | flops | bytes accessed | tf_op | source)
XLA Modules:
  0.0 191.2 jit_solution(15454084713056277438)
XLA Ops:
  0.6 0.0 copy-start.2
  0.7 0.1 pad.7.clone
  0.7 0.6 copy-done.2
  1.3 0.1 copy.17
  1.4 0.1 reshape.279
  1.5 0.1 reshape.278
  1.6 0.2 convert_reduce_fusion
  1.8 0.6 pad_add_fusion.slot_ref
  2.4 0.8 fusion.1
  3.2 0.1 broadcast_in_dim.51
  3.3 0.1 lt.50
  3.4 0.1 broadcast_in_dim.53
  3.4 0.1 mul.19
  3.5 0.7 add_add_fusion.ask_ref
  4.2 182.3 %shard_map.112 = (bf16[256,2048]{1,0:T(8,128)(2,1)}, bf16[256,2048]{1,0:T(8,128)(2,1)}, f32[512,256]{1,0:T(8,128)}) custom-call(s32[2,32]{1,0:T(2,128)} %pad_add_fusion.slot_ref, s32[4,8]{1,0:T(4,128)} %get-tuple-element.10.req_ref, s32[4,8,512]{2,1,0:T(8,128)} %add_add_fusion.ask_ref, bf16[1024,512]{1,0:T(8,128)(2,1)} %bitcast.4, bf16[1024,256]{1,0:T(8,128)(2,1)} %q_hbm.1, ...), custom_call_target="tpu_custom_call" | custom-call | tf_op jit(solution)/shard_map/pallas_call | solution.py:414
  186.6 0.0 copy-start
  186.6 2.4 %copy.23 = bf16[256,2048]{1,0:T(8,128)(2,1)} copy(bf16[256,2048]{1,0:T(8,128)(2,1)} %get-tuple-element.18) | data formatting | bytes 2097152
  189.0 0.0 copy-done
  189.0 0.0 copy-start.1
  189.0 1.0 copy.24
  190.0 0.4 copy-done.1
  190.4 0.8 copy.25
  (11 shorter events, 0.1 us)
Async XLA Ops:
  0.6 0.7 copy-start.2
  186.6 2.4 %copy-start = (bf16[256,2048]{1,0:T(8,128)(2,1)S(1)}, bf16[256,2048]{1,0:T(8,128)(2,1)}, u32[]{:S(2)}) copy-start(bf16[256,2048]{1,0:T(8,128)(2,1)} %get-tuple-element.7) | copy-start | bytes 3145732
  189.0 1.4 copy-start.1

commit v2 on v1

--- a/solution.py
+++ b/solution.py
@@ -100,6 +100,14 @@
     beside = remote(store_ref, rows.at[tp], gs.at[1, hi], gr.at[tp], mate)
     beside.start()
 
+    upper = st >= st_n // 2
+    mark = jnp.where(upper, st, st_n - 1 - st)
+
+    def far_peer(d):
+        i = d - 1
+        i = i + jnp.where(i >= mark, 1, 0)
+        return jnp.where(upper, i, st_n - 1 - i)
+
     def z_copy(phase, src, dst, peer):
         return remote(src, dst, zs.at[phase, peer], zr.at[phase, st], {"st": peer})
 
@@ -174,7 +182,7 @@
     lax.fori_loop(0, pass_rows // pass_len, low_step, 0)
 
     def kv_send(d, c):
-        peer = (st + d) % st_n
+        peer = far_peer(d)
         for k in range(depth):
             out[peer, k] = kv[ask_s[peer, 1, k]]
         z_copy(1, out.at[peer], inc.at[st], peer).start()
@@ -232,7 +240,7 @@
     lax.fori_loop(0, blocks, block_step, 0)
 
     def grad_send(d, c):
-        peer = (st + d) % st_n
+        peer = far_peer(d)
         z_copy(1, out.at[peer], inc.at[st], peer).wait_send()
         for k in range(depth):
             out[peer, k] = reqg[req_ref[peer, k]]
@@ -295,24 +303,25 @@
     scatter_first(0, gboth, wqg, tp_part, tp_pair, tok_pair)
     scatter_second(0, gboth, wqg, tp_part, tp_pair, tp_send, tp_recv, tok_pair)
 
+    def gather_sums(o, first):
+        def step(i, c):
+            r = pl.ds(pl.multiple_of(i * m_tile, m_tile), m_tile)
+            part = dot(hot[o, r, :], arr[o].reshape(hot_cols, 2 * cols))
+            acc[r] = part if first else acc[r] + part
+            return c
+
+        lax.fori_loop(0, pass_rows // m_tile, step, 0)
+
+    gather_sums(st, True)
+
     def grad_wait(d, c):
         peer = (st + d) % st_n
         z_wait(2, out.at[peer], arr.at[peer], peer)
+        gather_sums(peer, False)
         return c
 
     lax.fori_loop(1, st_n, grad_wait, 0)
-
-    def sum_step(i, c):
-        r = pl.ds(pl.multiple_of(i * m_tile, m_tile), m_tile)
-
-        def owner(o, total):
-            return total + dot(hot[o, r, :], arr[o].reshape(hot_cols, 2 * cols))
-
-        total = lax.fori_loop(0, st_n, owner, jnp.zeros((m_tile, 2 * cols), F32))
-        plow[r] = total.astype(BF)
-        return c
-
-    lax.fori_loop(0, pass_rows // m_tile, sum_step, 0)
+    plow[...] = acc[...].astype(BF)
 
     scatter_first(1, plow, wkv, sp_part, sp_pair, sto_pair)
 
@@ -329,7 +338,7 @@
         return dwp.at[pl.ds(pl.multiple_of(s * share, share), share), :]
 
     def wkey_send(d, c):
-        peer = (st + d) % st_n
+        peer = far_peer(d)
         z_copy(3, part_of(peer), dwr.at[st], peer).start()
         return c
 

time: 191 us -> 178 us (0.932)
  the two profiles are of different devices: /device:TPU:24 before, /device:TPU:15 now
where the time goes in v2:
time: 178 us; the launch traced here: 177 us
  Pallas kernels  169 us (95%)
  local copies, waits for them, and re-layouts  5.83 us (3%)
  other arithmetic  2.32 us (1%)
    pallas_call x1, Pallas kernels, local(): pl.pallas_call(functools.partial(kernel, st_n, tp_n, depth, pass_len), ou...  169 us
    unnamed x10, local copies, waits for them, and re-layouts  5.26 us

profile of v2, /device:TPU:15, one launch (start us, length us, event | category | flops | bytes accessed | tf_op | source)
XLA Modules:
  0.0 177.4 jit_solution(2458699354651219665)
XLA Ops:
  0.6 0.0 copy-start.2
  0.7 0.1 pad.7.clone
  0.7 0.6 copy-done.2
  1.3 0.1 copy.17
  1.4 0.1 reshape.279
  1.5 0.1 reshape.278
  1.6 0.2 convert_reduce_fusion
  1.8 0.6 pad_add_fusion.slot_ref
  2.4 0.8 fusion.1
  3.2 0.1 broadcast_in_dim.51
  3.3 0.1 lt.50
  3.4 0.1 broadcast_in_dim.53
  3.4 0.1 mul.19
  3.5 0.7 add_add_fusion.ask_ref
  4.2 168.5 %shard_map.112 = (bf16[256,2048]{1,0:T(8,128)(2,1)}, bf16[256,2048]{1,0:T(8,128)(2,1)}, f32[512,256]{1,0:T(8,128)}) custom-call(s32[2,32]{1,0:T(2,128)} %pad_add_fusion.slot_ref, s32[4,8]{1,0:T(4,128)} %get-tuple-element.10.req_ref, s32[4,8,512]{2,1,0:T(8,128)} %add_add_fusion.ask_ref, bf16[1024,512]{1,0:T(8,128)(2,1)} %bitcast.4, bf16[1024,256]{1,0:T(8,128)(2,1)} %q_hbm.1, ...), custom_call_target="tpu_custom_call" | custom-call | tf_op jit(solution)/shard_map/pallas_call | solution.py:423
  172.8 0.0 copy-start
  172.8 2.4 %copy.23 = bf16[256,2048]{1,0:T(8,128)(2,1)} copy(bf16[256,2048]{1,0:T(8,128)(2,1)} %get-tuple-element.18) | data formatting | bytes 2097152
  175.2 0.0 copy-done
  175.2 0.0 copy-start.1
  175.2 1.0 copy.24
  176.2 0.4 copy-done.1
  176.6 0.8 copy.25
  (11 shorter events, 0.1 us)
Async XLA Ops:
  0.6 0.7 copy-start.2
  172.8 2.4 %copy-start = (bf16[256,2048]{1,0:T(8,128)(2,1)S(1)}, bf16[256,2048]{1,0:T(8,128)(2,1)}, u32[]{:S(2)}) copy-start(bf16[256,2048]{1,0:T(8,128)(2,1)} %get-tuple-element.7) | copy-start | bytes 3145732
  175.2 1.4 copy-start.1

commit v3 on v2

--- a/solution.py
+++ b/solution.py
@@ -42,8 +42,8 @@
     st_n, tp_n, depth, pass_len,
     slot_ref, req_ref, ask_ref, store_ref, q_hbm, g_hbm, wq_hbm, wg_hbm, wk_hbm, wv_hbm, m_hbm,
     tok_out, store_out, wkey_out,
-    rows, wkv, wqg, q_v, g_v, m_v, acc, kv, ask_in, ask_s, out, inc, kvb, reqg, gboth, arr,
-    hot, plow, dwp, dwr, tp_part, tp_pair, tp_send, tp_recv, sp_part, sp_pair, sp_send, sp_recv,
+    rows, wkv, wqg, q_v, g_v, m_v, acc, kv, ask_in, ask_s, out, inc_k, inc_v, ret, prob_v, kvb, reqg, gboth, arr,
+    hot, plow, dwp, dwr, tp_part, tp_pair, tp_recv, sp_part, sp_pair, sp_recv,
     lsem, gs, gr, zs, zr, ps, pr, xs, xr,
 ):
     st = lax.axis_index("st")
@@ -181,34 +181,98 @@
 
     lax.fori_loop(0, pass_rows // pass_len, low_step, 0)
 
+    ks, vs_all = pl.ds(0, cols), pl.ds(cols, cols)
+
+    def half(ref, peer, part):
+        return ref.at[peer, :, :, part]
+
+    def key_copy(peer):
+        return z_copy(1, half(out, peer, ks), inc_k.at[st], peer)
+
+    def value_copy(peer):
+        return z_copy(4, half(out, peer, vs_all), inc_v.at[st], peer)
+
     def kv_send(d, c):
         peer = far_peer(d)
         for k in range(depth):
             out[peer, k] = kv[ask_s[peer, 1, k]]
-        z_copy(1, out.at[peer], inc.at[st], peer).start()
+        key_copy(peer).start()
+        return c
+
+    def value_send(d, c):
+        value_copy(far_peer(d)).start()
         return c
 
     lax.fori_loop(1, st_n, kv_send, 0)
+    lax.fori_loop(1, st_n, value_send, 0)
     for k in range(depth):
-        inc[st, k] = kv[ask_s[st, 1, k]]
+        picked = kv[ask_s[st, 1, k]]
+        inc_k[st, k] = picked[:, :cols]
+        inc_v[st, k] = picked[:, cols:]
     for copy in loads_q + loads_qg:
         copy.wait()
 
-    def kv_wait(d, c):
+    def key_wait(d, c):
         peer = (st + d) % st_n
-        z_wait(1, out.at[peer], inc.at[peer], peer)
-        return c
-
-    lax.fori_loop(1, st_n, kv_wait, 0)
-
+        z_wait(1, half(out, peer, ks), inc_k.at[peer], peer)
+        return c
+
+    lax.fori_loop(1, st_n, key_wait, 0)
     scale = HD ** (-0.5)
+
+    def probs_step(b, c):
+        r = pl.ds(pl.multiple_of(b * BLK, BLK), BLK)
+        for j in range(PB):
+            kvb[j * pass_len : (j + 1) * pass_len, :cols] = inc_k[
+                slot_ref[0, b * PB + j], slot_ref[1, b * PB + j]
+            ]
+        for head in range(heads):
+            hs = slice(head * HD, (head + 1) * HD)
+            vs = slice(cols + head * HD, cols + (head + 1) * HD)
+            gate = g_v[r, hs].astype(F32)
+            scores = dot(q_v[r, hs], kvb[:, hs], NT) * scale
+            shifted = jnp.exp(scores - jnp.max(scores, axis=-1, keepdims=True))
+            prob = shifted / jnp.sum(shifted, axis=-1, keepdims=True)
+            prob_v[head, r, :] = prob
+            sig = 1.0 / (1.0 + jnp.exp(-gate))
+            att_grad = (gate * sig * m_v[r, hs].astype(F32)).astype(BF)
+            value_grad = dot(prob.astype(BF), att_grad, TN).astype(BF)
+            for j in range(PB):
+                reqg[b * PB + j, :, vs] = value_grad[j * pass_len : (j + 1) * pass_len]
+        return c
+
+    lax.fori_loop(0, blocks, probs_step, 0)
+
+    def back_copy(phase, part, peer):
+        return z_copy(phase, half(ret, peer, part), half(arr, st, part), peer)
+
+    def give_back(phase, part, span):
+        def send(d, c):
+            peer = far_peer(d)
+            for k in range(depth):
+                ret[peer, k, :, span] = reqg[req_ref[peer, k]][:, span]
+            back_copy(phase, part, peer).start()
+            return c
+
+        lax.fori_loop(1, st_n, send, 0)
+        for k in range(depth):
+            arr[st, k, :, span] = reqg[req_ref[st, k]][:, span]
+
+    give_back(2, vs_all, slice(cols, 2 * cols))
+
+    def value_wait(d, c):
+        peer = (st + d) % st_n
+        z_wait(4, half(out, peer, vs_all), inc_v.at[peer], peer)
+        return c
+
+    lax.fori_loop(1, st_n, value_wait, 0)
 
     def block_step(b, c):
         r = pl.ds(pl.multiple_of(b * BLK, BLK), BLK)
         for j in range(PB):
-            kvb[j * pass_len : (j + 1) * pass_len, :] = inc[
-                slot_ref[0, b * PB + j], slot_ref[1, b * PB + j]
-            ]
+            o, k = slot_ref[0, b * PB + j], slot_ref[1, b * PB + j]
+            kvb[j * pass_len : (j + 1) * pass_len, :cols] = inc_k[o, k]
+            kvb[j * pass_len : (j + 1) * pass_len, cols:] = inc_v[o, k]
         for head in range(heads):
             hs = slice(head * HD, (head + 1) * HD)
             vs = slice(cols + head * HD, cols + (head + 1) * HD)
@@ -217,11 +281,8 @@
             value = kvb[:, vs]
             gate = g_v[r, hs].astype(F32)
             grad = m_v[r, hs].astype(F32)
-            scores = dot(q, key, NT) * scale
-            shifted = jnp.exp(scores - jnp.max(scores, axis=-1, keepdims=True))
-            prob = shifted / jnp.sum(shifted, axis=-1, keepdims=True)
-            low = prob.astype(BF)
-            attended = dot(low, value)
+            prob = prob_v[head, r, :]
+            attended = dot(prob.astype(BF), value)
             sig = 1.0 / (1.0 + jnp.exp(-gate))
             att_grad = (gate * sig * grad).astype(BF)
             gboth[r, vs] = (grad * attended * sig * (1.0 + gate * (1.0 - sig))).astype(BF)
@@ -230,26 +291,12 @@
             score_grad = (scale * prob * (prob_grad - inner)).astype(BF)
             gboth[r, hs] = dot(score_grad, key).astype(BF)
             key_grad = dot(score_grad, q, TN).astype(BF)
-            value_grad = dot(low, att_grad, TN).astype(BF)
             for j in range(PB):
-                js = slice(j * pass_len, (j + 1) * pass_len)
-                reqg[b * PB + j, :, hs] = key_grad[js]
-                reqg[b * PB + j, :, vs] = value_grad[js]
+                reqg[b * PB + j, :, hs] = key_grad[j * pass_len : (j + 1) * pass_len]
         return c
 
     lax.fori_loop(0, blocks, block_step, 0)
-
-    def grad_send(d, c):
-        peer = far_peer(d)
-        z_copy(1, out.at[peer], inc.at[st], peer).wait_send()
-        for k in range(depth):
-            out[peer, k] = reqg[req_ref[peer, k]]
-        z_copy(2, out.at[peer], arr.at[st], peer).start()
-        return c
-
-    lax.fori_loop(1, st_n, grad_send, 0)
-    for k in range(depth):
-        arr[st, k] = reqg[req_ref[st, k]]
+    give_back(5, ks, slice(0, cols))
 
     n_tile = tile_of(model, 512)
 
@@ -275,7 +322,7 @@
 
     def cross(which, send, recv, h):
         return remote(
-            send.at[h], recv.at[hi], xs.at[which, h], xr.at[which, hi], {"tp": h * 2 + lo}
+            send.at[h * 2 + lo], recv.at[hi], xs.at[which, h], xr.at[which, hi], {"tp": h * 2 + lo}
         )
 
     def scatter_second(which, src, weight, part, pair, send, recv, pair_rows):
@@ -284,14 +331,14 @@
             expand(src, weight, part, pair_rows, h * 2 + lo)
             pair_copy(which, part, pair, h).wait_recv()
             if d < hi_n:
-                send[h] = (part[h * 2 + lo].astype(F32) + pair[h].astype(F32)).astype(BF)
-                cross(which, send, recv, h).start()
+                part[h * 2 + lo] = (part[h * 2 + lo].astype(F32) + pair[h].astype(F32)).astype(BF)
+                cross(which, part, recv, h).start()
 
     def scatter_last(which, part, pair, send, recv, result):
         for d in range(1, hi_n):
             h = (hi + d) % hi_n
             remote(
-                send.at[h], recv.at[h], xs.at[which, h], xr.at[which, h], {"tp": h * 2 + lo}
+                send.at[h * 2 + lo], recv.at[h], xs.at[which, h], xr.at[which, h], {"tp": h * 2 + lo}
             ).wait_recv()
         total = part[tp].astype(F32) + pair[hi].astype(F32)
         for d in range(1, hi_n):
@@ -301,27 +348,28 @@
     tok_pair = tok_rows // tp_n
     sto_pair = pass_rows // tp_n
     scatter_first(0, gboth, wqg, tp_part, tp_pair, tok_pair)
-    scatter_second(0, gboth, wqg, tp_part, tp_pair, tp_send, tp_recv, tok_pair)
-
-    def gather_sums(o, first):
+    scatter_second(0, gboth, wqg, tp_part, tp_pair, tp_part, tp_recv, tok_pair)
+
+    def gather_sums(o, span, first):
         def step(i, c):
             r = pl.ds(pl.multiple_of(i * m_tile, m_tile), m_tile)
-            part = dot(hot[o, r, :], arr[o].reshape(hot_cols, 2 * cols))
-            acc[r] = part if first else acc[r] + part
+            part = dot(hot[o, r, :], arr[o, :, :, span].reshape(hot_cols, cols))
+            acc[r, span] = part if first else acc[r, span] + part
             return c
 
         lax.fori_loop(0, pass_rows // m_tile, step, 0)
 
-    gather_sums(st, True)
-
-    def grad_wait(d, c):
-        peer = (st + d) % st_n
-        z_wait(2, out.at[peer], arr.at[peer], peer)
-        gather_sums(peer, False)
-        return c
-
-    lax.fori_loop(1, st_n, grad_wait, 0)
-    plow[...] = acc[...].astype(BF)
+    for phase, part, span in ((2, vs_all, slice(cols, 2 * cols)), (5, ks, slice(0, cols))):
+        gather_sums(st, span, True)
+
+        def grad_wait(d, c):
+            peer = (st + d) % st_n
+            z_wait(phase, half(ret, peer, part), half(arr, peer, part), peer)
+            gather_sums(peer, span, False)
+            return c
+
+        lax.fori_loop(1, st_n, grad_wait, 0)
+        plow[:, span] = acc[:, span].astype(BF)
 
     scatter_first(1, plow, wkv, sp_part, sp_pair, sto_pair)
 
@@ -343,8 +391,8 @@
         return c
 
     lax.fori_loop(1, st_n, wkey_send, 0)
-    scatter_second(1, plow, wkv, sp_part, sp_pair, sp_send, sp_recv, sto_pair)
-    scatter_last(0, tp_part, tp_pair, tp_send, tp_recv, tok_out)
+    scatter_second(1, plow, wkv, sp_part, sp_pair, sp_part, sp_recv, sto_pair)
+    scatter_last(0, tp_part, tp_pair, tp_part, tp_recv, tok_out)
     wkey_out[...] = part_of(st)[...].astype(F32)
 
     def wkey_wait(d, c):
@@ -354,7 +402,7 @@
         return c
 
     lax.fori_loop(1, st_n, wkey_wait, 0)
-    scatter_last(1, sp_part, sp_pair, sp_send, sp_recv, store_out)
+    scatter_last(1, sp_part, sp_pair, sp_part, sp_recv, store_out)
 
     for copy in across + [beside] + onward:
         copy.wait_send()
@@ -362,7 +410,10 @@
     def drain(d, c):
         peer = (st + d) % st_n
         z_copy(0, ask_ref.at[peer], ask_in.at[st], peer).wait_send()
-        z_copy(2, out.at[peer], arr.at[st], peer).wait_send()
+        key_copy(peer).wait_send()
+        value_copy(peer).wait_send()
+        back_copy(2, vs_all, peer).wait_send()
+        back_copy(5, ks, peer).wait_send()
         z_copy(3, part_of(peer), dwr.at[st], peer).wait_send()
         return c
 
@@ -372,8 +423,8 @@
         pair_copy(0, tp_part, tp_pair, h).wait_send()
         pair_copy(1, sp_part, sp_pair, h).wait_send()
         if d < hi_n:
-            cross(0, tp_send, tp_recv, h).wait_send()
-            cross(1, sp_send, sp_recv, h).wait_send()
+            cross(0, tp_part, tp_recv, h).wait_send()
+            cross(1, sp_part, sp_recv, h).wait_send()
 
 
 def local(pass_ids, store, queries, gate_pre, w_query, w_gate, w_key, w_value, d_mem):
@@ -441,7 +492,10 @@
             V((st_n, 8, width), jnp.int32),
             pltpu.SMEM((st_n, 8, width), jnp.int32),
             V((st_n, depth, pass_len, pair), BF),
+            V((st_n, depth, pass_len, cols), BF),
+            V((st_n, depth, pass_len, cols), BF),
             V((st_n, depth, pass_len, pair), BF),
+            V((cols // HD, tok_rows, PB * pass_len), F32),
             V((PB * pass_len, pair), BF),
             V((requests, pass_len, pair), BF),
             V((tok_rows, pair), BF),
@@ -453,16 +507,14 @@
             V((tp_n, tok_pair, model), BF),
             V((hi_n, tok_pair, model), BF),
             V((hi_n, tok_pair, model), BF),
-            V((hi_n, tok_pair, model), BF),
             V((tp_n, sto_pair, model), BF),
-            V((hi_n, sto_pair, model), BF),
             V((hi_n, sto_pair, model), BF),
             V((hi_n, sto_pair, model), BF),
             DMA((9,)),
             DMA((3, hi_n)),
             DMA((tp_n,)),
-            DMA((4, st_n)),
-            DMA((4, st_n)),
+            DMA((6, st_n)),
+            DMA((6, st_n)),
             DMA((2, hi_n)),
             DMA((2, hi_n)),
             DMA((2, hi_n)),

time: 178 us -> 168 us (0.944)
  Pallas kernels: 169 us -> 158 us
    pallas_call x1, Pallas kernels: 169 us -> 158 us  [local(): pl.pallas_call(functools.partial(kernel, st_n, tp_n, depth, pass_len), ou...]
where the time goes in v3:
time: 168 us; the launch traced here: 167 us
  Pallas kernels  158 us (94%)
  local copies, waits for them, and re-layouts  5.83 us (3%)
  other arithmetic  2.32 us (1%)
    pallas_call x1, Pallas kernels, local(): pl.pallas_call(functools.partial(kernel, st_n, tp_n, depth, pass_len), ou...  158 us
    unnamed x10, local copies, waits for them, and re-layouts  5.26 us

profile of v3, /device:TPU:15, one launch (start us, length us, event | category | flops | bytes accessed | tf_op | source)
XLA Modules:
  0.0 167.4 jit_solution(11189842651473927074)
XLA Ops:
  0.6 0.0 copy-start.2
  0.7 0.1 pad.7.clone
  0.7 0.6 copy-done.2
  1.3 0.1 copy.17
  1.4 0.1 reshape.279
  1.5 0.1 reshape.278
  1.6 0.2 convert_reduce_fusion
  1.8 0.6 pad_add_fusion.slot_ref
  2.4 0.8 fusion.1
  3.2 0.1 broadcast_in_dim.51
  3.3 0.1 lt.50
  3.4 0.1 broadcast_in_dim.53
  3.4 0.1 mul.19
  3.5 0.7 add_add_fusion.ask_ref
  4.2 158.5 %shard_map.112 = (bf16[256,2048]{1,0:T(8,128)(2,1)}, bf16[256,2048]{1,0:T(8,128)(2,1)}, f32[512,256]{1,0:T(8,128)}) custom-call(s32[2,32]{1,0:T(2,128)} %pad_add_fusion.slot_ref, s32[4,8]{1,0:T(4,128)} %get-tuple-element.10.req_ref, s32[4,8,512]{2,1,0:T(8,128)} %add_add_fusion.ask_ref, bf16[1024,512]{1,0:T(8,128)(2,1)} %bitcast.4, bf16[1024,256]{1,0:T(8,128)(2,1)} %q_hbm.1, ...), custom_call_target="tpu_custom_call" | custom-call | tf_op jit(solution)/shard_map/pallas_call | solution.py:474
  162.8 0.0 copy-start
  162.8 2.4 %copy.23 = bf16[256,2048]{1,0:T(8,128)(2,1)} copy(bf16[256,2048]{1,0:T(8,128)(2,1)} %get-tuple-element.18) | data formatting | bytes 2097152
  165.2 0.0 copy-done
  165.2 0.0 copy-start.1
  165.2 1.0 copy.24
  166.1 0.4 copy-done.1
  166.6 0.8 copy.25
  (11 shorter events, 0.1 us)
Async XLA Ops:
  0.6 0.7 copy-start.2
  162.8 2.4 %copy-start = (bf16[256,2048]{1,0:T(8,128)(2,1)S(1)}, bf16[256,2048]{1,0:T(8,128)(2,1)}, u32[]{:S(2)}) copy-start(bf16[256,2048]{1,0:T(8,128)(2,1)} %get-tuple-element.7) | copy-start | bytes 3145732
  165.2 1.4 copy-start.1
